TPU v7x, 32 devices: a whole 2x2x4 slice. The times are simulated.
32 devices in a mesh: sp: 4 (over z), fs: 4 (over y, x), tp: 2 (over core).
Axes of the slice: x: 2, y: 2, z: 4, core: 2. Of those that a mesh axis runs over, the one named last changes fastest.
Arguments:
- tokens: bfloat16 [4, 2048, 2048], P('fs', 'sp'), may hold values from -6 to 6
- input_gain: float32 [2048], replicated, may hold values from 0.1 to 1.9
- weight_gate: bfloat16 [2048, 2048], P('sp', 'tp'), may hold values from -0.125 to 0.125
- weight_input: bfloat16 [2048, 2048], P('sp', 'tp'), may hold values from -0.125 to 0.125
- weight_write: bfloat16 [2048, 1024], P('sp', 'tp'), may hold values from -0.125 to 0.125
- weight_read: bfloat16 [2048, 1024], P('sp', 'tp'), may hold values from -0.125 to 0.125
- weight_step: bfloat16 [2048, 32], P('sp', 'tp'), may hold values from -0.125 to 0.125
- weight_value: bfloat16 [2048, 2048], P('sp', 'tp'), may hold values from -0.125 to 0.125
- weight_sigmoid: bfloat16 [2048, 2048], P('sp', 'tp'), may hold values from -0.125 to 0.125
- filter_input: bfloat16 [4, 2048], P(None, 'tp'), may hold values from -3 to 3
- filter_write: bfloat16 [4, 1024], P(None, 'tp'), may hold values from -3 to 3
- filter_read: bfloat16 [4, 1024], P(None, 'tp'), may hold values from -3 to 3
- step_bias: float32 [32], P('tp'), may hold values from -4.5 to -3.5
- rate_log: float32 [32], P('tp'), as said below
- skip_gain: float32 [32], P('tp'), may hold values from 0.1 to 1.9
- output_gain: float32 [2048], P('tp'), may hold values from 0.1 to 1.9
- opening_state: float32 [4, 32, 64, 128], P('fs', 'tp'), may hold values from -12 to 12
- decay_shift: float32 [4, 32, 2048], P('fs', 'tp', 'sp'), may hold values from -3 to 0, as said below
- depth_filter: bfloat16 [31, 2048], P(None, 'tp'), may hold values from -40 to 40
- channel_gain: float32 [2048], P('tp'), may hold values from 0.1 to 1.9
- unproject_state: bfloat16 [2048, 2048], P('tp', 'sp'), may hold values from -0.09375 to 0.09375
- unproject_filter: bfloat16 [2048, 2048], P('tp', 'sp'), may hold values from -0.09375 to 0.09375
Outputs:
- mixed: bfloat16 [4, 2048, 2048], P('fs', ('sp', 'tp'))
Inputs may be any that keep to these rules, and one draw needn't show every extreme that they name: `rate_log`: logarithms of the heads' decay rates. `decay_shift`: Non-positive.
All inputs are finite; a program needn't handle non-finite values.
Results may differ from a plain program's by a relative error of at most 0.018.
Values may be sent and summed in bfloat16 or wider, within the bound.
A program may use at most 128 MiB of HBM per device.

v0:
```python
from functools import partial

import jax
import jax.numpy as jnp
from jax import lax
from jax.sharding import PartitionSpec as P

HEAD_DIM = 64
STATE = 128
CM = 2048
BLOCK = 128


exact_mode = lax.Precision.HIGHEST


def passed_along(array, axis, by):
    length = lax.axis_size(axis)
    pairs = [(i, i + by) for i in range(length) if 0 <= i + by < length]
    return lax.ppermute(array, axis, pairs)


def carried_in(array, axis, combine, identity):
    length, here = (lax.axis_size(axis), lax.axis_index(axis))
    everything = jax.tree.map(
        lambda part, kind: lax.all_gather(part.astype(kind), axis),
        array,
        (jnp.bfloat16, jnp.bfloat16),
    )
    start = jax.tree.map(
        lambda part, zero: jnp.broadcast_to(jnp.asarray(zero, part.dtype), part.shape),
        array,
        identity,
    )

    def lap(k, before):
        reached = k < here
        new = combine(
            before, jax.tree.map(lambda part, own: part[k].astype(own.dtype), everything, array)
        )
        return jax.tree.map(lambda a, b: jnp.where(reached, a, b), new, before)

    return lax.fori_loop(0, length, lap, start)


def causal_filter(border, values, kernel):
    extended = jnp.concatenate([border, values], axis=0).astype(jnp.float32)
    weights = kernel.astype(jnp.float32)
    row_count = values.shape[0]
    result = jnp.zeros(values.shape, jnp.float32)
    for offset in range(kernel.shape[0]):
        result = result + weights[offset] * extended[offset : offset + row_count]
    return result


def block_step(direct_gain, memory, pieces):
    input_block, write_block, read_block, step_block, log_block = pieces
    head_count = input_block.shape[1]
    per_group = head_count // write_block.shape[1]
    running = jnp.cumsum(log_block, axis=0)
    write_heads = jnp.repeat(write_block, per_group, axis=1)
    read_heads = jnp.repeat(read_block, per_group, axis=1)
    scores = jnp.einsum("lhn,shn->hls", read_heads, write_heads, precision=exact_mode)
    spread = running.T[:, :, None] - running.T[:, None, :]
    row_index = lax.broadcasted_iota(jnp.int32, spread.shape, 1)
    col_index = lax.broadcasted_iota(jnp.int32, spread.shape, 2)
    decays = jnp.exp(jnp.where(row_index >= col_index, spread, -jnp.inf))
    scaled_inputs = input_block * step_block[:, :, None]
    inside = jnp.einsum("hls,shp->lhp", scores * decays, scaled_inputs, precision=exact_mode)
    carried = jnp.exp(running)[:, :, None] * jnp.einsum(
        "lhn,hpn->lhp", read_heads, memory, precision=exact_mode
    )
    output = inside + carried + direct_gain[None, :, None] * input_block
    to_end = jnp.exp(running[-1][None, :] - running)
    fresh_terms = jnp.einsum(
        "lhp,lhn->hpn", scaled_inputs * to_end[:, :, None], write_heads, precision=exact_mode
    )
    new_memory = jnp.exp(running[-1])[:, None, None] * memory + fresh_terms
    return (new_memory, output)


def per_device(
    tokens,
    input_gain,
    weight_gate,
    weight_input,
    weight_write,
    weight_read,
    weight_step,
    weight_value,
    weight_sigmoid,
    filter_input,
    filter_write,
    filter_read,
    step_bias,
    rate_log,
    skip_gain,
    output_gain,
    opening_state,
    decay_shift,
    depth_filter,
    channel_gain,
    unproject_state,
    unproject_filter,
):
    row_count = tokens.shape[1]
    source = tokens[0].astype(jnp.float32)
    normed = (
        source * lax.rsqrt(jnp.mean(source * source, axis=-1, keepdims=True) + 1e-06) * input_gain
    ).astype(jnp.bfloat16)
    pieces = (
        lax.all_gather(weight_gate, "sp", axis=0, tiled=True),
        lax.all_gather(weight_input, "sp", axis=0, tiled=True),
        lax.all_gather(weight_write, "sp", axis=0, tiled=True),
        lax.all_gather(weight_read, "sp", axis=0, tiled=True),
        lax.all_gather(weight_step, "sp", axis=0, tiled=True),
        lax.all_gather(weight_value, "sp", axis=0, tiled=True),
        lax.all_gather(weight_sigmoid, "sp", axis=0, tiled=True),
    )
    sums = tuple((jnp.dot(normed, piece, preferred_element_type=jnp.float32) for piece in pieces))
    gate_values, input_values, write_values, read_values, step_values, value_rows, sigmoid_rows = (
        total.astype(jnp.bfloat16) for total in sums
    )
    glu_rows = (
        value_rows.astype(jnp.float32) * jax.nn.sigmoid(sigmoid_rows.astype(jnp.float32))
    ).astype(jnp.bfloat16)
    short_rim = filter_input.shape[0] - 1
    long_rim = depth_filter.shape[0] - 1
    borders = passed_along(
        (
            input_values[row_count - short_rim :],
            write_values[row_count - short_rim :],
            read_values[row_count - short_rim :],
            glu_rows[row_count - long_rim :],
        ),
        "sp",
        1,
    )
    mixed_input = jax.nn.silu(causal_filter(borders[0], input_values, filter_input)).astype(
        jnp.bfloat16
    )
    mixed_write = jax.nn.silu(causal_filter(borders[1], write_values, filter_write)).astype(
        jnp.bfloat16
    )
    mixed_read = jax.nn.silu(causal_filter(borders[2], read_values, filter_read)).astype(
        jnp.bfloat16
    )
    head_count = rate_log.shape[0]
    group_count = mixed_write.shape[1] // STATE
    step_sizes = jax.nn.softplus(step_values.astype(jnp.float32) + step_bias)
    log_rates = -step_sizes * jnp.exp(rate_log) + decay_shift[0].T
    inputs_float = mixed_input.astype(jnp.float32).reshape(row_count, head_count, HEAD_DIM)
    write_float = mixed_write.astype(jnp.float32).reshape(row_count, group_count, STATE)
    read_float = mixed_read.astype(jnp.float32).reshape(row_count, group_count, STATE)
    block_count = row_count // BLOCK
    blocked = tuple(
        (
            array.reshape((block_count, BLOCK) + array.shape[1:])
            for array in (inputs_float, write_float, read_float, step_sizes, log_rates)
        )
    )
    zero_memory = jnp.zeros((head_count, HEAD_DIM, STATE), jnp.float32)
    local_memory, outputs = lax.scan(partial(block_step, skip_gain), zero_memory, blocked)
    outputs = outputs.reshape(row_count, head_count, HEAD_DIM)
    running = jnp.cumsum(log_rates, axis=0)
    total_decay = running[-1]

    def combine(earlier, later):
        return (earlier[0] + later[0], earlier[1] * jnp.exp(later[0])[:, None, None] + later[1])

    before, leading_memory = carried_in(
        (total_decay, local_memory),
        "sp",
        combine,
        (jnp.zeros_like(total_decay), jnp.zeros_like(local_memory)),
    )
    entering = opening_state[0] * jnp.exp(before)[:, None, None] + leading_memory
    read_heads = jnp.repeat(read_float, head_count // group_count, axis=1)
    outputs = outputs + jnp.exp(running)[:, :, None] * jnp.einsum(
        "lhn,hpn->lhp", read_heads, entering, precision=exact_mode
    )
    gated = outputs.reshape(row_count, -1) * jax.nn.silu(gate_values.astype(jnp.float32))
    grouped = gated.reshape(row_count, group_count, -1)
    grouped = grouped * lax.rsqrt(jnp.mean(grouped * grouped, axis=-1, keepdims=True) + 1e-06)
    state_out = (grouped.reshape(row_count, -1) * output_gain).astype(jnp.bfloat16)
    filtered = causal_filter(borders[3], glu_rows, depth_filter)
    channel_sums = lax.psum((jnp.sum(filtered, axis=1), jnp.sum(filtered * filtered, axis=1)), "tp")
    mean_value = channel_sums[0] / CM
    mean_square = channel_sums[1] / CM
    variance = mean_square - mean_value * mean_value
    normal_rows = (
        (filtered - mean_value[:, None]) * lax.rsqrt(variance + 1e-05)[:, None] * channel_gain
    )
    filter_out = jax.nn.silu(normal_rows).astype(jnp.bfloat16)
    full_state, full_filter = (
        lax.all_gather(unproject_state, "sp", axis=1, tiled=True),
        lax.all_gather(unproject_filter, "sp", axis=1, tiled=True),
    )
    summed = lax.psum_scatter(
        (
            jnp.dot(state_out, full_state, preferred_element_type=jnp.float32)
            + jnp.dot(filter_out, full_filter, preferred_element_type=jnp.float32)
        ).astype(jnp.bfloat16),
        "tp",
        scatter_dimension=0,
        tiled=True,
    )
    return summed[None]


def solution(mesh):
    in_specs = (
        P("fs", "sp", None),
        P(),
        P("sp", "tp"),
        P("sp", "tp"),
        P("sp", "tp"),
        P("sp", "tp"),
        P("sp", "tp"),
        P("sp", "tp"),
        P("sp", "tp"),
        P(None, "tp"),
        P(None, "tp"),
        P(None, "tp"),
        P("tp"),
        P("tp"),
        P("tp"),
        P("tp"),
        P("fs", "tp", None, None),
        P("fs", "tp", "sp"),
        P(None, "tp"),
        P("tp"),
        P("tp", "sp"),
        P("tp", "sp"),
    )
    out_specs = P("fs", ("sp", "tp"), None)
    return jax.shard_map(
        per_device, mesh=mesh, in_specs=in_specs, out_specs=out_specs, check_vma=False
    )
```

profile of v0, /device:TPU:0, one launch (start us, length us, event | category | flops | bytes accessed | tf_op | source)
XLA Modules:
  0.0 641.8 jit_solution(15246610743525412421)
XLA Ops:
  10.7 15.1 %all_gather.37 = bf16[2048,16]{0,1:T(8,128)(2,1)S(1)} all-gather(bf16[512,16]{0,1:T(8,128)(2,1)S(1)} %copy-done.13), channel_id=1, replica_groups=mesh['sp'=4,'fs'=4,'tp'=2] {'sp'}, dimensions={0}, use_global_device_ids=true | all-gather | bytes 81920 | tf_op jit(solution)/shard_map/all_gather | solution.py:116
  27.4 30.2 %all-gather.16.cloned.1.call-done = bf16[2048,512]{1,0:T(8,128)(2,1)} async-done(((bf16[512,512]{1,0:T(8,128)(2,1)}), bf16[2048,512]{1,0:T(8,128)(2,1)}) %all-gather.16.cloned.1.call-update) | async-done | bytes 2097168 | tf_op jit(solution)/shard_map/all_gather | solution.py:115
  62.4 41.1 %all-gather.14.cloned.1.call-done = bf16[2048,512]{1,0:T(8,128)(2,1)} async-done(((bf16[512,512]{1,0:T(8,128)(2,1)}), bf16[2048,512]{1,0:T(8,128)(2,1)}) %all-gather.14.cloned.1.call-update) | async-done | bytes 2097168 | tf_op jit(solution)/shard_map/all_gather | solution.py:114
  110.0 74.7 %all-gather.12.cloned.1.call-done = bf16[2048,1024]{1,0:T(8,128)(2,1)} async-done(((bf16[512,1024]{1,0:T(8,128)(2,1)}), bf16[2048,1024]{1,0:T(8,128)(2,1)}) %all-gather.12.cloned.1.call-update) | async-done | bytes 4194320 | tf_op jit(solution)/shard_map/all_gather | solution.py:113
  184.7 5.2 convolution_convert_fusion.3
  200.0 4.1 copy.107
  204.1 120.4 %while.29 = (s32[]{:T(128)}, f32[16,64,128]{2,1,0:T(8,128)}, f32[4,128,16,64]{1,0,3,2:T(4,128)}, f32[4,128,16]{2,1,0:T(8,128)}, f32[4,128,16,64]{1,3,2,0:T(8,128...) while((s32[]{:T(128)}, f32[16,64,128]{2,1,0:T(8,128)}, ...), condition=%wide.region_3.4_spmd.clone, body=%wide.region_1.3_spmd.clone.sunk | while | flops 1009385472 | bytes 16942680 | solution.py:163
  208.9 4.0 convolution_bitcast_fusion.3
  212.9 4.1 fusion.142
  217.1 13.9 %dynamic_update_slice.6 = f32[4,128,16,64]{1,0,3,2:T(4,128)} dynamic-update-slice(f32[4,128,16,64]{1,0,3,2:T(4,128)} %get-tuple-element.483, f32[1,128,16,64]{1,0,3,2:T(1,128)} %bitcast.241, s32[]{:T(128)} %get-tuple-element.481, s32[]{:T(128)} %constant.75.clone.1..sunk, s32[]{:T(128)} %constant.75.clone.1..sunk, s32[]{:T(128)} %constant.75.clone.1..sunk) | dynamic-update-slice | bytes 1048580 | tf_op jit(solution)/shard_map/while/body/jit(dynamic_update_index_in_dim)/dynamic_update_slice | solution.py:163
  238.7 4.0 convolution_bitcast_fusion.3
  242.8 4.3 fusion.142
  247.1 13.8 %dynamic_update_slice.6 = f32[4,128,16,64]{1,0,3,2:T(4,128)} dynamic-update-slice(f32[4,128,16,64]{1,0,3,2:T(4,128)} %get-tuple-element.483, f32[1,128,16,64]{1,0,3,2:T(1,128)} %bitcast.241, s32[]{:T(128)} %get-tuple-element.481, s32[]{:T(128)} %constant.75.clone.1..sunk, s32[]{:T(128)} %constant.75.clone.1..sunk, s32[]{:T(128)} %constant.75.clone.1..sunk) | dynamic-update-slice | bytes 1048580 | tf_op jit(solution)/shard_map/while/body/jit(dynamic_update_index_in_dim)/dynamic_update_slice | solution.py:163
  268.8 4.0 convolution_bitcast_fusion.3
  272.9 4.4 fusion.142
  277.3 13.8 %dynamic_update_slice.6 = f32[4,128,16,64]{1,0,3,2:T(4,128)} dynamic-update-slice(f32[4,128,16,64]{1,0,3,2:T(4,128)} %get-tuple-element.483, f32[1,128,16,64]{1,0,3,2:T(1,128)} %bitcast.241, s32[]{:T(128)} %get-tuple-element.481, s32[]{:T(128)} %constant.75.clone.1..sunk, s32[]{:T(128)} %constant.75.clone.1..sunk, s32[]{:T(128)} %constant.75.clone.1..sunk) | dynamic-update-slice | bytes 1048580 | tf_op jit(solution)/shard_map/while/body/jit(dynamic_update_index_in_dim)/dynamic_update_slice | solution.py:163
  299.1 4.0 convolution_bitcast_fusion.3
  303.2 4.3 fusion.142
  307.5 13.9 %dynamic_update_slice.6 = f32[4,128,16,64]{1,0,3,2:T(4,128)} dynamic-update-slice(f32[4,128,16,64]{1,0,3,2:T(4,128)} %get-tuple-element.483, f32[1,128,16,64]{1,0,3,2:T(1,128)} %bitcast.241, s32[]{:T(128)} %get-tuple-element.481, s32[]{:T(128)} %constant.75.clone.1..sunk, s32[]{:T(128)} %constant.75.clone.1..sunk, s32[]{:T(128)} %constant.75.clone.1..sunk) | dynamic-update-slice | bytes 1048580 | tf_op jit(solution)/shard_map/while/body/jit(dynamic_update_index_in_dim)/dynamic_update_slice | solution.py:163
  330.4 12.3 %all-gather.1 = bf16[4,1,16]{2,1,0:T(2,128)(2,1)S(1)} all-gather(bf16[1,1,16]{2,1,0:T(2,128)(2,1)S(1)} %bitcast.302), channel_id=1, replica_groups=mesh['sp'=4,'fs'=4,'tp'=2] {'sp'}, dimensions={0}, use_global_device_ids=true | all-gather | bytes 160 | tf_op jit(solution)/shard_map/all_gather | solution.py:26
  342.8 5.2 convolution_convert_fusion.1
  348.0 5.4 multiply_convert_fusion.1
  359.0 10.8 %fusion.95 = (f32[512]{0:T(512)S(1)}, f32[512]{0:T(512)S(1)}, f32[512,1024]{1,0:T(8,128)}) fusion(f32[542,1024]{1,0:T(8,128)S(1)} %maximum_convert_fusion, f32[1024]{0:T(1024)S(1)} %bitcast.296, f32[1024]{0:T(1024)S(1)} %bitcast.295, f32[1024]{0:T(1024)S(1)} %bitcast.294, f32[1024]{0:T(1024)S(1)} %bitcast.293, f32[1024]{0:T(1024)S(1)} %bitcast.292, ...), kind=kLoop, calls=%fused_computation.193 | loop fusion | flops 33553408 | bytes 67239936 | tf_op jit(solution)/shard_map/reduce_sum | solution.py:187
  374.0 4.5 while.30
  380.3 6.2 fusion.57
  389.5 67.6 %all-gather.18.cloned.1.call-done = bf16[2048,1024]{1,0:T(8,128)(2,1)} async-done(((bf16[512,1024]{1,0:T(8,128)(2,1)}), bf16[2048,1024]{1,0:T(8,128)(2,1)}) %all-gather.18.cloned.1.call-update) | async-done | bytes 4194320 | tf_op jit(solution)/shard_map/all_gather | solution.py:112
  457.1 7.6 %fusion.103 = (f32[512,1024]{1,0:T(8,128)}, f32[512,1024]{1,0:T(8,128)}) fusion(f32[512,1024]{1,0:T(8,128)} %copy.116, bf16[2048,1024]{1,0:T(8,128)(2,1)} %all-gather.18.cloned.1.call-done, bf16[1,512,2048]{2,1,0:T(8,128)(2,1)S(1)} %copy-done.4, f32[2048]{0:T(1024)S(1)} %copy-done.17, f32[512]{0:T(512)S(1)} %add_rsqrt_fusion.2), kind=kOutput, calls=%fused_computation.200 | convolution fusion | flops 2155872256 | bytes 12593152 | tf_op jit(solution)/shard_map/dot_general | solution.py:120
  470.4 67.6 %all-gather.20.cloned.1.call-done = bf16[1024,2048]{1,0:T(8,128)(2,1)} async-done(((bf16[1024,512]{1,0:T(8,128)(2,1)}), bf16[1024,2048]{1,0:T(8,128)(2,1)}) %all-gather.20.cloned.1.call-update) | async-done | bytes 4194320 | tf_op jit(solution)/shard_map/all_gather | solution.py:196
  537.9 7.9 %fusion.60 = f32[512,2048]{1,0:T(8,128)} fusion(bf16[1024,2048]{1,0:T(8,128)(2,1)} %all-gather.20.cloned.1.call-done, f32[512,1024]{1,0:T(8,128)} %get-tuple-element.364, f32[512,1024]{1,0:T(8,128)} %bitcast.248, f32[1024]{0:T(1024)S(1)} %copy-done.18), kind=kOutput, calls=%fused_computation.135 | convolution fusion | flops 2149056512 | bytes 12587008 | tf_op jit(solution)/shard_map/dot_general | solution.py:201
  545.8 72.9 %all-gather.26.cloned.1.call-done = bf16[1024,2048]{1,0:T(8,128)(2,1)} async-done(((bf16[1024,512]{1,0:T(8,128)(2,1)}), bf16[1024,2048]{1,0:T(8,128)(2,1)}) %all-gather.26.cloned.1.call-update) | async-done | bytes 4194320 | tf_op jit(solution)/shard_map/all_gather | solution.py:197
  618.8 7.6 %add_convert_fusion = bf16[512,2048]{1,0:T(8,128)(2,1)} fusion(f32[512,2048]{1,0:T(8,128)} %fusion.60, bf16[1024,2048]{1,0:T(8,128)(2,1)} %all-gather.26.cloned.1.call-done, f32[512,1024]{1,0:T(8,128)S(1)} %copy-done.2, f32[1024]{0:T(1024)S(1)} %copy-done.19, f32[512]{0:T(512)S(1)} %get-tuple-element.361, f32[512]{0:T(512)S(1)} %get-tuple-element.360), kind=kOutput, calls=%fused_computation.42 | convolution fusion | flops 2153775104 | bytes 12591104 | tf_op jit(solution)/shard_map/dot_general | solution.py:202
  626.3 8.4 %reduce-scatter.2.cloned.1.call-done = bf16[256,2048]{1,0:T(8,128)(2,1)} async-done(((bf16[512,2048]{1,0:T(8,128)(2,1)}), bf16[256,2048]{1,0:T(8,128)(2,1)}) %reduce-scatter.2.cloned.1.call-update) | async-done | bytes 1048592 | tf_op jit(solution)/shard_map/reduce_scatter | solution.py:199
  (201 shorter events, 88.9 us)
Async XLA Ops:
  6.5 3.5 copy-start.3
  6.5 51.0 %all-gather.16.cloned.1.call-start = ((), (), s32[]{:S(2)}) async-start(), calls=%async_computation.3 | async-start | bytes 2621440 | tf_op jit(solution)/shard_map/all_gather | solution.py:115
  7.3 96.3 %all-gather.14.cloned.1.call-start = ((), (), s32[]{:S(2)}) async-start(), calls=%async_computation.2 | async-start | bytes 2621440 | tf_op jit(solution)/shard_map/all_gather | solution.py:114
  8.0 176.7 %all-gather.12.cloned.1.call-start = ((), (), s32[]{:S(2)}) async-start(), calls=%async_computation.1 | async-start | bytes 5242880 | tf_op jit(solution)/shard_map/all_gather | solution.py:113
  8.7 1.8 copy-start.14
  8.8 1.8 copy-start.12
  8.8 1.9 copy-start.15
  8.8 1.9 copy-start.20
  8.8 1.9 copy-start.13
  8.8 17.0 %copy-start.11 = (f32[1,16,512]{2,1,0:T(8,128)S(1)}, f32[1,16,512]{2,1,0:T(8,128)}, u32[]{:S(2)}) copy-start(f32[1,16,512]{2,1,0:T(8,128)} %param.43) | copy-start | bytes 98308
  8.8 17.0 %copy-start.17 = (f32[2048]{0:T(1024)S(1)}, f32[2048]{0:T(1024)}, u32[]{:S(2)}) copy-start(f32[2048]{0:T(1024)} %param.27) | copy-start | bytes 24580
  8.8 17.0 %copy-start.21 = (f32[16]{0:T(128)S(1)}, f32[16]{0:T(128)}, u32[]{:S(2)}) copy-start(f32[16]{0:T(128)} %param.38) | copy-start | bytes 196
  8.8 333.9 %all-gather.22.cloned.1.call-start = ((), (), s32[]{:S(2)}) async-start(), calls=%async_computation.6 | async-start | bytes 5242880 | tf_op jit(solution)/shard_map/all_gather | solution.py:117
  9.4 338.6 %all-gather.24.cloned.1.call-start = ((), (), s32[]{:S(2)}) async-start(), calls=%async_computation.7 | async-start | bytes 5242880 | tf_op jit(solution)/shard_map/all_gather | solution.py:118
  10.0 364.0 %all-gather.28.cloned.1.call-start = ((), (), s32[]{:S(2)}) async-start(), calls=%async_computation.10 | async-start | bytes 1310720 | tf_op jit(solution)/shard_map/all_gather | solution.py:26
  60.5 48.1 %collective-permute-start.2 = (bf16[3,512]{1,0:T(4,128)(2,1)S(1)}, bf16[3,512]{1,0:T(4,128)(2,1)S(1)}, u32[]{:S(2)}, u32[]{:S(2)}) collective-permute-start(bf16[3,512]{1,0:T(4,128)(2,1)S(1)} %slice.398), channel_id=1, source_target_pairs={{0,8},{8,16},{16,24},{1,9},{9,17},{17,25},{2,10},{10,18},{18,26},{... | collective-permute-start | bytes 9224 | tf_op jit(solution)/shard_map/ppermute | solution.py:20
  106.5 3.4 collective-permute-start.1
  190.0 5.8 collective-permute-start
  200.0 4.1 copy-start.16
  324.5 4.2 copy-start.10
  326.3 130.8 %all-gather.18.cloned.1.call-start = ((), (), s32[]{:S(2)}) async-start(), calls=%async_computation.4 | async-start | bytes 5242880 | tf_op jit(solution)/shard_map/all_gather | solution.py:112
  327.1 210.8 %all-gather.20.cloned.1.call-start = ((), (), s32[]{:S(2)}) async-start(), calls=%async_computation.5 | async-start | bytes 5242880 | tf_op jit(solution)/shard_map/all_gather | solution.py:196
  327.8 290.9 %all-gather.26.cloned.1.call-start = ((), (), s32[]{:S(2)}) async-start(), calls=%async_computation.8 | async-start | bytes 5242880 | tf_op jit(solution)/shard_map/all_gather | solution.py:197
  328.5 306.2 %reduce-scatter.2.cloned.1.call-start = ((), (), s32[]{:S(2)}) async-start(), calls=%async_computation.9 | async-start | bytes 3145728 | tf_op jit(solution)/shard_map/reduce_scatter | solution.py:199
  353.5 2.0 copy-start.5
  353.5 5.2 collective-permute-start.3
  355.4 3.3 copy-start.6
  378.6 1.7 copy-start.9
  386.4 70.6 %copy-start.4 = (bf16[1,512,2048]{2,1,0:T(8,128)(2,1)S(1)}, bf16[1,512,2048]{2,1,0:T(8,128)(2,1)}, u32[]{:S(2)}) copy-start(bf16[1,512,2048]{2,1,0:T(8,128)(2,1)} %param.26) | copy-start | bytes 6291460
  468.5 69.4 %copy-start.18 = (f32[1024]{0:T(1024)S(1)}, f32[1024]{0:T(1024)}, u32[]{:S(2)}) copy-start(f32[1024]{0:T(1024)} %param.41) | copy-start | bytes 12292
  537.9 80.8 %copy-start.2 = (f32[512,1024]{1,0:T(8,128)S(1)}, f32[512,1024]{1,0:T(8,128)}, u32[]{:S(2)}) copy-start(f32[512,1024]{1,0:T(8,128)} %get-tuple-element.306) | copy-start | bytes 6291460
  537.9 80.8 %copy-start.19 = (f32[1024]{0:T(1024)S(1)}, f32[1024]{0:T(1024)}, u32[]{:S(2)}) copy-start(f32[1024]{0:T(1024)} %param.45) | copy-start | bytes 12292
  (4 other events, 5.9 us)
Sparse Core Ops, SparseCore 0:
  8.9 48.6 all-gather.15
  59.1 44.3 all-gather.13
  105.1 79.5 all-gather.11
  186.1 79.2 all-gather.21
  266.8 79.2 all-gather.23
  347.5 26.4 all-gather.27
  375.6 81.4 all-gather.17
  458.7 79.2 all-gather.19
  539.5 79.2 all-gather.25
  626.5 8.2 reduce-scatter.1
where the time goes:
time: 649 us; the launch traced here: 642 us
  waiting for transfers between devices  370 us (57%)
  matrix products  106 us (16%)
  local copies, waits for them, and re-layouts  88.5 us (14%)
  blocking collectives  30.1 us (5%)
  other arithmetic  25.3 us (4%)
  between operations  14.3 us (2%)
  starting transfers between devices  7.24 us (1%)
    all_gather x1, waiting for transfers between devices, per_device(): lax.all_gather(weight_input, 'sp', axis=0, tiled=True)  74.7 us
    all_gather x1, waiting for transfers between devices, per_device(): lax.all_gather(unproject_filter, 'sp', axis=1, tiled=True)  72.9 us
    all_gather x1, waiting for transfers between devices, per_device(): lax.all_gather(weight_gate, 'sp', axis=0, tiled=True)  67.6 us
    all_gather x1, waiting for transfers between devices, per_device(): lax.all_gather(unproject_state, 'sp', axis=1, tiled=True)  67.6 us
    dynamic_update_slice x4, local copies, waits for them, and re-layouts, per_device(): lax.scan(partial(block_step, skip_gain), zero_memory, blocked)  55.4 us
    all_gather x1, waiting for transfers between devices, per_device(): lax.all_gather(weight_write, 'sp', axis=0, tiled=True)  41.1 us
    all_gather x1, waiting for transfers between devices, per_device(): lax.all_gather(weight_read, 'sp', axis=0, tiled=True)  30.2 us
    dot_general x7, matrix products, per_device(): jnp.dot(normed, piece, preferred_element_type=jnp.float32)  30 us
  transfers between devices with their start and end apart: 14, of which 9 were waited for; matrix products, arithmetic and copies ran while one was open for 33% of the time, Pallas kernels for 0%

commit v1 on v0

v1 whole, which is shorter than its diff:
```python
import jax
import jax.numpy as jnp
from jax import lax
from jax.experimental import pallas as pl
from jax.experimental.pallas import tpu as pltpu
from jax.sharding import PartitionSpec as P

HEAD_DIM = 64
STATE = 128
CM = 2048
BLOCK = 128


def passed_along(array, axis, by):
    length = lax.axis_size(axis)
    pairs = [(i, i + by) for i in range(length) if 0 <= i + by < length]
    return lax.ppermute(array, axis, pairs)


def causal_filter(border, values, kernel):
    extended = jnp.concatenate([border, values], axis=0).astype(jnp.float32)
    weights = kernel.astype(jnp.float32)
    row_count = values.shape[0]
    result = jnp.zeros(values.shape, jnp.float32)
    for offset in range(kernel.shape[0]):
        result = result + weights[offset] * extended[offset : offset + row_count]
    return result


def gathered(pieces):
    share = lax.axis_size("fs")
    cut = []
    for piece in pieces:
        rows = piece.shape[0] // share
        cut.append(lax.dynamic_slice_in_dim(piece, lax.axis_index("fs") * rows, rows, 0))
    joined = cut[0] if len(cut) == 1 else jnp.concatenate(cut, axis=1)
    return lax.all_gather(joined, ("sp", "fs"), axis=0, tiled=True)


def over_lanes(columns, width):
    rows, count = columns.shape
    lane = lax.broadcasted_iota(jnp.int32, (rows, width), 1) // HEAD_DIM
    result = jnp.broadcast_to(columns[:, 0:1], (rows, width))
    for head in range(1, count):
        result = jnp.where(lane == head, columns[:, head : head + 1], result)
    return result


def local_kernel(
    x_ref, write_ref, read_ref, col_ref, end_ref, row_ref, step_ref, y_ref, state_ref
):
    rows, width = x_ref.shape
    heads = col_ref.shape[2]
    state = jnp.zeros((STATE, width), jnp.float32)
    row_at = lax.broadcasted_iota(jnp.int32, (BLOCK, BLOCK), 0)
    col_at = lax.broadcasted_iota(jnp.int32, (BLOCK, BLOCK), 1)
    lane = lax.broadcasted_iota(jnp.int32, (BLOCK, width), 1) // HEAD_DIM
    for block in range(rows // BLOCK):
        at = pl.ds(block * BLOCK, BLOCK)
        x, write, read = x_ref[at, :], write_ref[at, :], read_ref[at, :]
        columns = col_ref[0, at, :]
        scores = lax.dot_general(
            read, write, (((1,), (1,)), ((), ())), preferred_element_type=jnp.float32
        )
        weights, inputs = [], []
        for head in range(heads):
            spread = columns[:, head : head + 1] - row_ref[0, head : head + 1, at]
            decay = jnp.exp(jnp.where(row_at >= col_at, spread, -jnp.inf))
            weights.append((scores * decay * step_ref[0, head : head + 1, at]).astype(jnp.bfloat16))
            inputs.append(jnp.where(lane == head, x, jnp.zeros_like(x)))
        inside = jnp.dot(
            jnp.concatenate(weights, axis=1),
            jnp.concatenate(inputs, axis=0),
            preferred_element_type=jnp.float32,
        )
        grown = over_lanes(jnp.exp(columns), width)
        if block:
            inside = inside + grown * jnp.dot(
                read, state.astype(jnp.bfloat16), preferred_element_type=jnp.float32
            )
        y_ref[at, :] = inside
        scaled = (x.astype(jnp.float32) * over_lanes(end_ref[0, at, :], width)).astype(jnp.bfloat16)
        fresh = lax.dot_general(
            write, scaled, (((0,), (0,)), ((), ())), preferred_element_type=jnp.float32
        )
        state = state * grown[BLOCK - 1 :, :] + fresh
    state_ref[...] = state


def finish_kernel(
    y_ref, x_ref, read_ref, gate_ref, enter_ref, col_ref, skip_ref, gain_ref, out_ref
):
    rows, width = x_ref.shape
    entering = enter_ref[...].astype(jnp.bfloat16)
    for block in range(rows // BLOCK):
        at = pl.ds(block * BLOCK, BLOCK)
        carried = jnp.dot(read_ref[at, :], entering, preferred_element_type=jnp.float32)
        total = y_ref[at, :] + over_lanes(col_ref[0, at, :], width) * carried
        total = total + skip_ref[...] * x_ref[at, :].astype(jnp.float32)
        gate = gate_ref[at, :].astype(jnp.float32)
        gated = total * (gate * jax.nn.sigmoid(gate))
        size = jnp.mean(gated * gated, axis=1, keepdims=True)
        out_ref[at, :] = (gated * lax.rsqrt(size + 1e-06) * gain_ref[...]).astype(jnp.bfloat16)


def per_device(
    tokens,
    input_gain,
    weight_gate,
    weight_input,
    weight_write,
    weight_read,
    weight_step,
    weight_value,
    weight_sigmoid,
    filter_input,
    filter_write,
    filter_read,
    step_bias,
    rate_log,
    skip_gain,
    output_gain,
    opening_state,
    decay_shift,
    depth_filter,
    channel_gain,
    unproject_state,
    unproject_filter,
):
    row_count = tokens.shape[1]
    length = lax.axis_size("sp")
    head_count = rate_log.shape[0]
    width = weight_input.shape[1]
    group_count = weight_write.shape[1] // STATE
    per_group = head_count // group_count
    group_width = per_group * HEAD_DIM
    source = tokens[0].astype(jnp.float32)
    normed = (
        source * lax.rsqrt(jnp.mean(source * source, axis=-1, keepdims=True) + 1e-06) * input_gain
    ).astype(jnp.bfloat16)

    def project(weight):
        return jnp.dot(normed, weight, preferred_element_type=jnp.float32).astype(jnp.bfloat16)

    mixer_rows = project(gathered((weight_input, weight_write, weight_read, weight_step)))
    glu_pair = project(gathered((weight_value, weight_sigmoid)))
    gate_values = project(gathered((weight_gate,)))
    mixer_width = width + 2 * group_count * STATE
    step_values = mixer_rows[:, mixer_width:]
    mixer_rows = mixer_rows[:, :mixer_width]
    short_rim = filter_input.shape[0] - 1
    long_rim = depth_filter.shape[0] - 1
    mixed = jax.nn.silu(
        causal_filter(
            passed_along(mixer_rows[row_count - short_rim :], "sp", 1),
            mixer_rows,
            jnp.concatenate([filter_input, filter_write, filter_read], axis=1),
        )
    ).astype(jnp.bfloat16)
    step_sizes = jax.nn.softplus(step_values.astype(jnp.float32) + step_bias)
    log_rates = -step_sizes * jnp.exp(rate_log) + decay_shift[0].T
    block_count = row_count // BLOCK
    blocked = jnp.cumsum(log_rates.reshape(block_count, BLOCK, head_count), axis=1)
    block_ends = blocked[:, -1]
    before = jnp.cumsum(block_ends, axis=0) - block_ends
    total_decay = before[-1] + block_ends[-1]
    to_end = jnp.exp(block_ends[:, None] - blocked).reshape(row_count, head_count) * step_sizes
    leading = jnp.exp(blocked + before[:, None]).reshape(row_count, head_count)
    blocked = blocked.reshape(row_count, head_count)

    def as_columns(array):
        return array.reshape(row_count, group_count, per_group).transpose(1, 0, 2)

    def as_rows(array):
        return array.T.reshape(group_count, per_group, row_count)

    wide = pl.BlockSpec((row_count, group_width), lambda g: (0, g))
    write_at, read_at = (width // STATE, width // STATE + group_count)
    write_spec = pl.BlockSpec((row_count, STATE), lambda g: (0, write_at + g))
    read_spec = pl.BlockSpec((row_count, STATE), lambda g: (0, read_at + g))
    column_spec = pl.BlockSpec((1, row_count, per_group), lambda g: (g, 0, 0))
    row_spec = pl.BlockSpec((1, per_group, row_count), lambda g: (g, 0, 0))
    state_spec = pl.BlockSpec((STATE, group_width), lambda g: (0, g))
    line_spec = pl.BlockSpec((1, group_width), lambda g: (0, g))
    local_rows, local_state = pl.pallas_call(
        local_kernel,
        grid=(group_count,),
        in_specs=[wide, write_spec, read_spec, column_spec, column_spec, row_spec, row_spec],
        out_specs=[wide, state_spec],
        out_shape=[
            jax.ShapeDtypeStruct((row_count, width), jnp.float32),
            jax.ShapeDtypeStruct((STATE, width), jnp.float32),
        ],
        cost_estimate=pl.CostEstimate(
            flops=8 * row_count * width * BLOCK, bytes_accessed=8 * row_count * width, transcendentals=0
        ),
    )(
        mixed,
        mixed,
        mixed,
        as_columns(blocked),
        as_columns(to_end),
        as_rows(blocked),
        as_rows(step_sizes),
    )
    decay_line = jnp.repeat(total_decay, HEAD_DIM)[None]
    decay_high = decay_line.astype(jnp.bfloat16)
    decay_low = (decay_line - decay_high.astype(jnp.float32)).astype(jnp.bfloat16)
    payload = jnp.concatenate(
        [
            local_state.astype(jnp.bfloat16),
            decay_high,
            decay_low,
            jnp.zeros((14, width), jnp.bfloat16),
        ],
        axis=0,
    )
    entering, reach = (jnp.zeros((STATE, width), jnp.float32), jnp.zeros((1, width), jnp.float32))
    for distance in range(1, length):
        earlier = passed_along(payload, "sp", distance).astype(jnp.float32)
        entering = entering + jnp.exp(reach) * earlier[:STATE]
        reach = reach + earlier[STATE : STATE + 1] + earlier[STATE + 1 : STATE + 2]
    opening = opening_state[0].reshape(width, STATE).T
    entering = entering + jnp.exp(reach) * opening
    state_out = pl.pallas_call(
        finish_kernel,
        grid=(group_count,),
        in_specs=[wide, wide, read_spec, wide, state_spec, column_spec, line_spec, line_spec],
        out_specs=wide,
        out_shape=jax.ShapeDtypeStruct((row_count, width), jnp.bfloat16),
        cost_estimate=pl.CostEstimate(
            flops=2 * row_count * width * STATE, bytes_accessed=10 * row_count * width, transcendentals=0
        ),
    )(
        local_rows,
        mixed,
        mixed,
        gate_values,
        entering,
        as_columns(leading),
        jnp.repeat(skip_gain, HEAD_DIM)[None],
        output_gain[None],
    )
    channels = weight_value.shape[1]
    glu_rows = (
        glu_pair[:, :channels].astype(jnp.float32)
        * jax.nn.sigmoid(glu_pair[:, channels:].astype(jnp.float32))
    ).astype(jnp.bfloat16)
    filtered = causal_filter(
        passed_along(glu_rows[row_count - long_rim :], "sp", 1), glu_rows, depth_filter
    )
    channel_sums = lax.psum((jnp.sum(filtered, axis=1), jnp.sum(filtered * filtered, axis=1)), "tp")
    mean_value = channel_sums[0] / CM
    mean_square = channel_sums[1] / CM
    variance = mean_square - mean_value * mean_value
    normal_rows = (
        (filtered - mean_value[:, None]) * lax.rsqrt(variance + 1e-05)[:, None] * channel_gain
    )
    filter_out = jax.nn.silu(normal_rows).astype(jnp.bfloat16)
    share = lax.axis_size("fs")
    piece_rows = unproject_state.shape[0] // share
    first = lax.axis_index("fs") * piece_rows
    piece = jnp.concatenate(
        [
            lax.dynamic_slice_in_dim(unproject_state, first, piece_rows, 0),
            lax.dynamic_slice_in_dim(unproject_filter, first, piece_rows, 0),
        ],
        axis=0,
    )
    output_maps = lax.all_gather(piece, ("sp", "fs"), axis=0, tiled=True)
    output_maps = output_maps.reshape(length, share * 2 * piece_rows, piece.shape[1])
    joined = jnp.concatenate(
        [
            part[:, i * piece_rows : (i + 1) * piece_rows]
            for i in range(share)
            for part in (state_out, filter_out)
        ],
        axis=1,
    )
    partial_rows = jnp.concatenate(
        [
            jnp.dot(joined, output_maps[i], preferred_element_type=jnp.float32).astype(jnp.bfloat16)
            for i in range(length)
        ],
        axis=1,
    )
    summed = lax.psum_scatter(partial_rows, "tp", scatter_dimension=0, tiled=True)
    return summed[None]


def solution(mesh):
    in_specs = (
        P("fs", "sp", None),
        P(),
        P("sp", "tp"),
        P("sp", "tp"),
        P("sp", "tp"),
        P("sp", "tp"),
        P("sp", "tp"),
        P("sp", "tp"),
        P("sp", "tp"),
        P(None, "tp"),
        P(None, "tp"),
        P(None, "tp"),
        P("tp"),
        P("tp"),
        P("tp"),
        P("tp"),
        P("fs", "tp", None, None),
        P("fs", "tp", "sp"),
        P(None, "tp"),
        P("tp"),
        P("tp", "sp"),
        P("tp", "sp"),
    )
    out_specs = P("fs", ("sp", "tp"), None)
    return jax.shard_map(
        per_device, mesh=mesh, in_specs=in_specs, out_specs=out_specs, check_vma=False
    )
```

time: 649 us -> 475 us (0.73); the launches traced: 642 us -> 474 us
  matrix products: 106 us -> 30 us
  local copies, waits for them, and re-layouts: 88.5 us -> 28.5 us
  blocking collectives: 30.1 us -> 2.65 us
  waiting for transfers between devices: 370 us -> 343 us
  Pallas kernels: 0 us -> 13.7 us
    dot_general x26 -> x7, matrix products: 106 us -> 30 us  [the longest x3 23.1 us: project(): jnp.dot(normed, weight, preferred_element_type=jnp.float32)]
    all_gather x9 -> x4, waiting for transfers between devices: 356 us -> 299 us  [the longest x3 269 us: gathered(): return lax.all_gather(joined, ('sp', 'fs'), axis=0, tiled=True)]
    dynamic_update_slice x4 -> x0, local copies, waits for them, and re-layouts: 55.4 us -> none  [per_device(): lax.scan(partial(block_step, skip_gain), zero_memory, blocked)]
    all_gather x2 -> x0, blocking collectives: 27.4 us -> none  [the longest x1 15.1 us: per_device(): lax.all_gather(weight_step, 'sp', axis=0, tiled=True)]
    ppermute x4 -> x5, waiting for transfers between devices: 0.51 us -> 26.6 us  [passed_along(): return lax.ppermute(array, axis, pairs)]
    pallas_call x0 -> x2, Pallas kernels: none -> 13.7 us  [the longest x1 7.25 us: per_device(): pl.pallas_call(local_kernel, grid=(group_count,), in_specs=[wide, write_s...]
    reduce_scatter x1, waiting for transfers between devices: 8.4 us -> 17.4 us  [per_device(): lax.psum_scatter(partial_rows, 'tp', scatter_dimension=0, tiled=True)]
  transfers between devices with their start and end apart: 14 -> 10, of which waited for: 9 -> 8; matrix products, arithmetic and copies ran while one was open for 33% -> 16% of each run, Pallas kernels for 0% -> 3%
where the time goes in v1:
time: 475 us; the launch traced here: 474 us
  waiting for transfers between devices  343 us (72%)
  other arithmetic  30.6 us (6%)
  matrix products  30 us (6%)
  local copies, waits for them, and re-layouts  28.5 us (6%)
  Pallas kernels  13.7 us (3%)
  between operations  13.7 us (3%)
  starting transfers between devices  12.1 us (3%)
    all_gather x3, waiting for transfers between devices, gathered(): return lax.all_gather(joined, ('sp', 'fs'), axis=0, tiled=True)  269 us
    all_gather x1, waiting for transfers between devices, per_device(): output_maps = lax.all_gather(piece, ('sp', 'fs'), axis=0, tiled=True)  29.8 us
    ppermute x5, waiting for transfers between devices, passed_along(): return lax.ppermute(array, axis, pairs)  26.6 us
    dot_general x3, matrix products, project(): jnp.dot(normed, weight, preferred_element_type=jnp.float32)  23.1 us
    reduce_scatter x1, waiting for transfers between devices, per_device(): lax.psum_scatter(partial_rows, 'tp', scatter_dimension=0, tiled=True)  17.4 us
    ppermute x5, starting transfers between devices, passed_along(): return lax.ppermute(array, axis, pairs)  11.9 us
    reduce_sum x1, other arithmetic, per_device(): jnp.sum(filtered, axis=1)  9.99 us
  transfers between devices with their start and end apart: 10, of which 8 were waited for; matrix products, arithmetic and copies ran while one was open for 16% of the time, Pallas kernels for 3%

profile of v1, /device:TPU:0, one launch (start us, length us, event | category | flops | bytes accessed | tf_op | source)
XLA Modules:
  0.0 474.4 jit_solution(17721935851679269901)
XLA Ops:
  20.3 104.9 %all-gather.9.cloned.1.call-done = bf16[2048,2048]{1,0:T(8,128)(2,1)} async-done(((bf16[128,2048]{1,0:T(8,128)(2,1)}), bf16[2048,2048]{1,0:T(8,128)(2,1)}) %all-gather.9.cloned.1.call-update) | async-done | bytes 8388624 | tf_op jit(solution)/shard_map/all_gather | solution.py:37
  125.2 8.2 %convolution_convert_fusion.1 = bf16[512,2048]{1,0:T(8,128)(2,1)S(1)} fusion(bf16[2048,2048]{1,0:T(8,128)(2,1)} %all-gather.9.cloned.1.call-done, bf16[1,512,2048]{2,1,0:T(8,128)(2,1)S(1)} %copy-done.5, f32[2048]{0:T(1024)S(1)} %copy-done.25, f32[512]{0:T(512)S(1)} %add_rsqrt_fusion.1), kind=kOutput, calls=%fused_computation.14 | convolution fusion | flops 4300210176 | bytes 12593152 | tf_op jit(solution)/shard_map/dot_general | solution.py:143
  134.0 2.5 collective-permute-start.4
  136.5 65.4 %all-gather.7.cloned.1.call-done = bf16[2048,1024]{1,0:T(8,128)(2,1)} async-done(((bf16[128,1024]{1,0:T(8,128)(2,1)}), bf16[2048,1024]{1,0:T(8,128)(2,1)}) %all-gather.7.cloned.1.call-update) | async-done | bytes 4194320 | tf_op jit(solution)/shard_map/all_gather | solution.py:37
  202.0 5.6 %convolution_convert_fusion.2.gate_ref = bf16[512,1024]{1,0:T(8,128)(2,1)} fusion(bf16[2048,1024]{1,0:T(8,128)(2,1)} %all-gather.7.cloned.1.call-done, bf16[1,512,2048]{2,1,0:T(8,128)(2,1)S(1)} %copy-done.5, f32[2048]{0:T(1024)S(1)} %copy-done.25, f32[512]{0:T(512)S(1)} %add_rsqrt_fusion.1), kind=kOutput, calls=%fused_computation.89 | convolution fusion | flops 2152202240 | bytes 7350272 | tf_op jit(solution)/shard_map/dot_general | solution.py:143
  207.9 10.0 %fusion.68 = (f32[512]{0:T(512)S(1)}, f32[512]{0:T(512)S(1)}, f32[512,1024]{1,0:T(8,128)S(1)}) fusion(f32[542,1024]{1,0:T(8,128)S(1)} %maximum_convert_fusion.1, f32[1024]{0:T(1024)S(1)} %bitcast.126, f32[1024]{0:T(1024)S(1)} %bitcast.125, f32[1024]{0:T(1024)S(1)} %bitcast.124, f32[1024]{0:T(1024)S(1)} %bitcast.123, f32[1024]{0:T(1024)S(1)} %bitcast.122, ...), kind=kLoop, calls=%fused_computation.143 | loop fusion | flops 33553408 | bytes 67239936 | tf_op jit(solution)/shard_map/reduce_sum | solution.py:252
  217.9 2.7 all-reduce
  221.3 99.0 %all-gather.5.cloned.1.call-done = bf16[2048,2064]{1,0:T(8,128)(2,1)} async-done(((bf16[128,2064]{1,0:T(8,128)(2,1)}), bf16[2048,2064]{1,0:T(8,128)(2,1)}) %all-gather.5.cloned.1.call-update) | async-done | bytes 8454160 | tf_op jit(solution)/shard_map/all_gather | solution.py:37
  320.2 9.3 %convolution_convert_fusion = bf16[512,2064]{1,0:T(8,128)(2,1)S(1)} fusion(bf16[2048,2064]{1,0:T(8,128)(2,1)} %all-gather.5.cloned.1.call-done, bf16[1,512,2048]{2,1,0:T(8,128)(2,1)} %param.22, f32[2048]{0:T(1024)} %param.23, f32[512]{0:T(512)} %copy-done.20), kind=kOutput, calls=%fused_computation.2 | convolution fusion | flops 4333772800 | bytes 12675072 | tf_op jit(solution)/shard_map/dot_general | solution.py:143
  332.9 3.0 collective-permute-start
  335.9 1.3 reduce_window_sum.28
  338.6 1.4 broadcast_in_dim_reshape.6
  339.9 1.4 fusion.74
  341.3 1.7 fusion.61
  344.9 1.4 copy.53
  348.8 1.3 copy.51
  350.9 1.4 maximum_convert_fusion
  352.2 3.6 multiply_convert_fusion.x_ref.write_ref.read_ref
  355.8 7.3 %shard_map.208 = (f32[512,1024]{1,0:T(8,128)}, f32[128,1024]{1,0:T(8,128)}) custom-call(bf16[512,2048]{1,0:T(8,128)(2,1)} %multiply_convert_fusion.x_ref.write_ref.read_ref, bf16[512,2048]{1,0:T(8,128)(2,1)} %multiply_convert_fusion.x_ref.write_ref.read_ref, bf16[512,2048]{1,0:T(8,128)(2,1)} %multiply_convert_fusion.x_ref.write_ref.read_ref, ...), custom_call_target="tpu_custom_call" | custom-call | flops 536870912 | bytes 4194304 | tf_op jit(solution)/shard_map/pallas_call | solution.py:185
  364.3 3.2 collective-permute-start.1
  367.5 1.8 collective-permute-start.2
  369.3 1.5 collective-permute-start.3
  371.1 1.3 copy.59
  372.4 8.4 %collective-permute-done.1 = bf16[144,1024]{1,0:T(8,128)(2,1)S(1)} collective-permute-done((bf16[144,1024]{1,0:T(8,128)(2,1)S(1)}, bf16[144,1024]{1,0:T(8,128)(2,1)S(1)}, u32[]{:S(2)}, u32[]{:S(2)}) %collective-permute-start.1) | collective-permute-done | bytes 294944 | tf_op jit(solution)/shard_map/ppermute | solution.py:17
  380.8 7.5 %collective-permute-done.2 = bf16[144,1024]{1,0:T(8,128)(2,1)S(1)} collective-permute-done((bf16[144,1024]{1,0:T(8,128)(2,1)S(1)}, bf16[144,1024]{1,0:T(8,128)(2,1)S(1)}, u32[]{:S(2)}, u32[]{:S(2)}) %collective-permute-start.2) | collective-permute-done | bytes 294944 | tf_op jit(solution)/shard_map/ppermute | solution.py:17
  388.4 10.8 %collective-permute-done.3 = bf16[144,1024]{1,0:T(8,128)(2,1)S(1)} collective-permute-done((bf16[144,1024]{1,0:T(8,128)(2,1)S(1)}, bf16[144,1024]{1,0:T(8,128)(2,1)S(1)}, u32[]{:S(2)}, u32[]{:S(2)}) %collective-permute-start.3) | collective-permute-done | bytes 294944 | tf_op jit(solution)/shard_map/ppermute | solution.py:17
  400.3 6.4 %shard_map.209 = bf16[512,1024]{1,0:T(8,128)(2,1)} custom-call(f32[512,1024]{1,0:T(8,128)} %get-tuple-element.7.y_ref, bf16[512,2048]{1,0:T(8,128)(2,1)} %multiply_convert_fusion.x_ref.write_ref.read_ref, bf16[512,2048]{1,0:T(8,128)(2,1)} %multiply_convert_fusion.x_ref.write_ref.read_ref, bf16[512,1024]{1,0:T(8,128)(2,1)} %convolution_convert_fusion.2.gate_ref, ...), custom_call_target="tpu_custom_call" | custom-call | flops 134217728 | bytes 5242880 | tf_op jit(solution)/shard_map/pallas_call | solution.py:225
  409.0 29.8 %all-gather.11.cloned.1.call-done = bf16[8192,512]{1,0:T(8,128)(2,1)} async-done(((bf16[512,512]{1,0:T(8,128)(2,1)}), bf16[8192,512]{1,0:T(8,128)(2,1)}) %all-gather.11.cloned.1.call-update) | async-done | bytes 8388624 | tf_op jit(solution)/shard_map/all_gather | solution.py:270
  438.8 3.0 fusion.44
  446.8 1.5 pad_maximum_fusion
  448.3 17.4 %reduce-scatter.2.cloned.1.call-done = bf16[256,2048]{0,1:T(8,128)(2,1)} async-done(((bf16[512,2048]{0,1:T(8,128)(2,1)}), bf16[256,2048]{0,1:T(8,128)(2,1)}) %reduce-scatter.2.cloned.1.call-update) | async-done | bytes 1048592 | tf_op jit(solution)/shard_map/reduce_scatter | solution.py:287
  465.6 2.3 copy.60
  (135 shorter events, 34.8 us)
Async XLA Ops:
  6.5 118.6 %all-gather.9.cloned.1.call-start = ((), (), s32[]{:S(2)}) async-start(), calls=%async_computation.3 | async-start | bytes 8912896 | tf_op jit(solution)/shard_map/all_gather | solution.py:37
  8.6 193.4 %all-gather.7.cloned.1.call-start = ((), (), s32[]{:S(2)}) async-start(), calls=%async_computation.2 | async-start | bytes 4456448 | tf_op jit(solution)/shard_map/all_gather | solution.py:37
  9.4 310.9 %all-gather.5.cloned.1.call-start = ((), (), s32[]{:S(2)}) async-start(), calls=%async_computation.1 | async-start | bytes 9469952 | tf_op jit(solution)/shard_map/all_gather | solution.py:37
  12.2 4.4 copy-start.7
  13.1 4.5 copy-start.23
  13.1 5.9 %copy-start.5 = (bf16[1,512,2048]{2,1,0:T(8,128)(2,1)S(1)}, bf16[1,512,2048]{2,1,0:T(8,128)(2,1)}, u32[]{:S(2)}) copy-start(bf16[1,512,2048]{2,1,0:T(8,128)(2,1)} %param.22) | copy-start | bytes 6291460
  13.1 425.7 %all-gather.11.cloned.1.call-start = ((), (), s32[]{:S(2)}) async-start(), calls=%async_computation.4 | async-start | bytes 8912896 | tf_op jit(solution)/shard_map/all_gather | solution.py:270
  15.2 4.3 copy-start.15
  15.2 4.3 copy-start.17
  15.2 4.3 copy-start.18
  15.3 4.3 copy-start.8
  15.3 109.9 %copy-start.25 = (f32[2048]{0:T(1024)S(1)}, f32[2048]{0:T(1024)}, u32[]{:S(2)}) copy-start(f32[2048]{0:T(1024)} %param.23) | copy-start | bytes 24580
  15.3 450.3 %reduce-scatter.2.cloned.1.call-start = ((), (), s32[]{:S(2)}) async-start(), calls=%async_computation.5 | async-start | bytes 3145728 | tf_op jit(solution)/shard_map/reduce_scatter | solution.py:287
  19.5 182.4 %copy-start.20 = (f32[512]{0:T(512)}, f32[512]{0:T(512)S(1)}, u32[]{:S(2)}) copy-start(f32[512]{0:T(512)S(1)} %add_rsqrt_fusion.1) | copy-start | bytes 6148
  134.0 73.5 %collective-permute-start.4 = (bf16[30,1024]{1,0:T(8,128)(2,1)S(1)}, bf16[30,1024]{1,0:T(8,128)(2,1)S(1)}, u32[]{:S(2)}, u32[]{:S(2)}) collective-permute-start(bf16[30,1024]{1,0:T(8,128)(2,1)S(1)} %slice.433), channel_id=1, source_target_pairs={{0,8},{8,16},{16,24},{1,9},{9,17},{17,25},{2,10},{10,18},{18,26},{... | collective-permute-start | bytes 184328 | tf_op jit(solution)/shard_map/ppermute | solution.py:17
  207.8 12.7 %copy-start.16 = (f32[1024]{0:T(1024)S(1)}, f32[1024]{0:T(1024)}, u32[]{:S(2)}) copy-start(f32[1024]{0:T(1024)} %param.41) | copy-start | bytes 12292
  221.2 108.9 %copy-start.6 = (f32[1,16,512]{1,2,0:T(8,128)S(1)}, f32[1,16,512]{1,2,0:T(8,128)}, u32[]{:S(2)}) copy-start(f32[1,16,512]{1,2,0:T(8,128)} %copy.49) | copy-start | bytes 98308
  320.2 10.0 %copy-start.19 = (f32[16]{0:T(128)S(1)}, f32[16]{0:T(128)}, u32[]{:S(2)}) copy-start(f32[16]{0:T(128)} %param.34) | copy-start | bytes 196
  320.2 10.0 %copy-start.22 = (f32[16]{0:T(128)S(1)}, f32[16]{0:T(128)}, u32[]{:S(2)}) copy-start(f32[16]{0:T(128)} %exp.37) | copy-start | bytes 196
  329.5 13.5 %copy-start.2 = (bf16[512,2064]{1,0:T(8,128)(2,1)}, bf16[512,2064]{1,0:T(8,128)(2,1)S(1)}, u32[]{:S(2)}) copy-start(bf16[512,2064]{1,0:T(8,128)(2,1)S(1)} %convolution_convert_fusion) | copy-start | bytes 6340612
  332.9 17.9 %collective-permute-start = (bf16[3,2048]{1,0:T(4,128)(2,1)}, bf16[3,2048]{1,0:T(4,128)(2,1)}, u32[]{:S(2)}, u32[]{:S(2)}) collective-permute-start(bf16[3,2048]{1,0:T(4,128)(2,1)} %slice.408), channel_id=1, source_target_pairs={{0,8},{8,16},{16,24},{1,9},{9,17},{17,25},{2,10},{10,18},{18,26},{... | collective-permute-start | bytes 36872 | tf_op jit(solution)/shard_map/ppermute | solution.py:17
  343.7 7.1 %slice-start = ((bf16[512,2064]{1,0:T(8,128)(2,1)}), bf16[512,2048]{1,0:T(8,128)(2,1)S(1)}, s32[]{:S(2)}) async-start(bf16[512,2064]{1,0:T(8,128)(2,1)} %copy-done.2), calls=%async_computation.6 | async-start | bytes 4194304 | tf_op jit(solution)/shard_map/slice | solution.py:150
  355.8 8.3 %copy-start.13 = (bf16[1,1024]{1,0:T(2,128)(2,1)S(1)}, bf16[1,1024]{1,0:T(2,128)(2,1)}, u32[]{:S(2)}) copy-start(bf16[1,1024]{1,0:T(2,128)(2,1)} %get-tuple-element.54) | copy-start | bytes 6148
  355.8 8.4 %copy-start.14 = (bf16[1,1024]{1,0:T(2,128)(2,1)S(1)}, bf16[1,1024]{1,0:T(2,128)(2,1)}, u32[]{:S(2)}) copy-start(bf16[1,1024]{1,0:T(2,128)(2,1)} %get-tuple-element.55) | copy-start | bytes 6148
  355.8 8.4 %copy-start.21 = (bf16[144]{0:T(256)(128)(2,1)S(1)}, bf16[144]{0:T(256)(128)(2,1)}, u32[]{:S(2)}) copy-start(bf16[144]{0:T(256)(128)(2,1)} %pad.13.clone) | copy-start | bytes 868
  355.8 15.0 %copy-start.12 = (f32[4,16]{1,0:T(4,128)S(1)}, f32[4,16]{1,0:T(4,128)}, u32[]{:S(2)}) copy-start(f32[4,16]{1,0:T(4,128)} %reduce_window_sum.28) | copy-start | bytes 772
  364.3 35.0 %copy-start.4 = (f32[1024,128]{0,1:T(8,128)S(1)}, f32[1024,128]{0,1:T(8,128)}, u32[]{:S(2)}) copy-start(f32[1024,128]{0,1:T(8,128)} %copy.56) | copy-start | bytes 1572868
  364.3 16.5 %collective-permute-start.1 = (bf16[144,1024]{1,0:T(8,128)(2,1)S(1)}, bf16[144,1024]{1,0:T(8,128)(2,1)S(1)}, u32[]{:S(2)}, u32[]{:S(2)}) collective-permute-start(bf16[144,1024]{1,0:T(8,128)(2,1)S(1)} %maximum_maximum_fusion), channel_id=1, source_target_pairs={{0,8},{8,16},{16,24},{1,9},{9,17},{17,25},{2,10},{10,18},{18,26},{... | collective-permute-start | bytes 884744 | tf_op jit(solution)/shard_map/ppermute | solution.py:17
  367.5 20.9 %collective-permute-start.2 = (bf16[144,1024]{1,0:T(8,128)(2,1)S(1)}, bf16[144,1024]{1,0:T(8,128)(2,1)S(1)}, u32[]{:S(2)}, u32[]{:S(2)}) collective-permute-start(bf16[144,1024]{1,0:T(8,128)(2,1)S(1)} %maximum_maximum_fusion), channel_id=1, source_target_pairs={{0,16},{8,24},{1,17},{9,25},{2,18},{10,26},{3,19},{11,27},{4,20},{... | collective-permute-start | bytes 884744 | tf_op jit(solution)/shard_map/ppermute | solution.py:17
  369.3 29.8 %collective-permute-start.3 = (bf16[144,1024]{1,0:T(8,128)(2,1)S(1)}, bf16[144,1024]{1,0:T(8,128)(2,1)S(1)}, u32[]{:S(2)}, u32[]{:S(2)}) collective-permute-start(bf16[144,1024]{1,0:T(8,128)(2,1)S(1)} %maximum_maximum_fusion), channel_id=1, source_target_pairs={{0,24},{1,25},{2,26},{3,27},{4,28},{5,29},{6,30},{7,31}} | collective-permute-start | bytes 884744 | tf_op jit(solution)/shard_map/ppermute | solution.py:17
  438.8 4.0 copy-start.24
  448.2 19.7 %copy-start.1 = (bf16[512,1024]{1,0:T(8,128)(2,1)S(1)}, bf16[512,1024]{1,0:T(8,128)(2,1)}, u32[]{:S(2)}) copy-start(bf16[512,1024]{1,0:T(8,128)(2,1)} %param.24) | copy-start | bytes 3145732
  (6 other events, 14.1 us)
Sparse Core Ops, SparseCore 0:
  10.1 115.0 all-gather.8
  127.9 73.9 all-gather.6
  204.6 115.5 all-gather.4
  322.9 115.9 all-gather.10
  448.4 17.1 reduce-scatter.1

commit v2 on v1

--- a/solution.py
+++ b/solution.py
@@ -1,3 +1,5 @@
+from functools import partial
+
 import jax
 import jax.numpy as jnp
 from jax import lax
@@ -35,6 +37,117 @@
         cut.append(lax.dynamic_slice_in_dim(piece, lax.axis_index("fs") * rows, rows, 0))
     joined = cut[0] if len(cut) == 1 else jnp.concatenate(cut, axis=1)
     return lax.all_gather(joined, ("sp", "fs"), axis=0, tiled=True)
+
+
+def spread_kernel(
+    cuts, shard_ref, out_ref, z_send, z_recv, x_send, x_recv, y_send, y_recv,
+    u_send, u_recv, v_send, v_recv, own_sem,
+):
+    length, share = lax.axis_size("sp"), lax.axis_size("fs")
+    here, member, side = lax.axis_index("sp"), lax.axis_index("fs"), lax.axis_index("tp")
+    rows = shard_ref.shape[0]
+    part = rows // share
+    half = part // 2
+    beside = member + 1 - 2 * lax.rem(member, 2)
+    across = lax.rem(member + 2, share)
+    corner = lax.rem(beside + 2, share)
+    partners = [(lax.rem(here + k, length), member, side) for k in range(1, length)]
+    partners += [(here, beside, side), (here, across, side)]
+    barrier = pltpu.get_barrier_semaphore()
+    for partner in partners:
+        pl.semaphore_signal(
+            barrier, inc=1, device_id=partner, device_id_type=pl.DeviceIdType.MESH
+        )
+    pl.semaphore_wait(barrier, len(partners))
+
+    def place(start, size, cut):
+        return out_ref.at[pl.ds(pl.multiple_of(start, 16), size), pl.ds(*cut)]
+
+    def move(source, target, send, recv, device):
+        return pltpu.make_async_remote_copy(
+            src_ref=source, dst_ref=target, send_sem=send, recv_sem=recv,
+            device_id=device, device_id_type=pl.DeviceIdType.MESH,
+        )
+
+    items = [(c, k) for c in range(len(cuts)) for k in range(1, length)]
+    started = []
+    for c, k in items:
+        source = shard_ref.at[pl.ds(pl.multiple_of(member * part, 16), part), pl.ds(*cuts[c])]
+        copy = move(
+            source,
+            place(here * rows + member * part, part, cuts[c]),
+            z_send.at[c, k],
+            z_recv.at[c, k],
+            partners[k - 1],
+        )
+        copy.start()
+        started.append(copy)
+    own = pltpu.make_async_copy(
+        shard_ref, out_ref.at[pl.ds(pl.multiple_of(here * rows, 16), rows), :], own_sem
+    )
+    own.start()
+
+    def first_stage(c, k):
+        begin = lax.rem(here + length - k, length) * rows
+        spot = place(begin + member * part, part, cuts[c])
+        move(spot, spot, z_send.at[c, k], z_recv.at[c, k], partners[k - 1]).wait_recv()
+        for send, recv, device in ((x_send, x_recv, partners[-2]), (y_send, y_recv, partners[-1])):
+            copy = move(spot, spot, send.at[c, k], recv.at[c, k], device)
+            copy.start()
+            started.append(copy)
+
+    def second_stage(c, k):
+        begin = lax.rem(here + length - k, length) * rows
+        spot = place(begin + beside * part, part, cuts[c])
+        move(spot, spot, x_send.at[c, k], x_recv.at[c, k], partners[-2]).wait_recv()
+        low = place(begin + beside * part, half, cuts[c])
+        copy = move(low, low, u_send.at[c, k], u_recv.at[c, k], partners[-1])
+        copy.start()
+        started.append(copy)
+        spot = place(begin + across * part, part, cuts[c])
+        move(spot, spot, y_send.at[c, k], y_recv.at[c, k], partners[-1]).wait_recv()
+        high = place(begin + across * part + half, half, cuts[c])
+        copy = move(high, high, v_send.at[c, k], v_recv.at[c, k], partners[-2])
+        copy.start()
+        started.append(copy)
+
+    for at, (c, k) in enumerate(items):
+        first_stage(c, k)
+        if at:
+            second_stage(*items[at - 1])
+    second_stage(*items[-1])
+    for c, k in items:
+        begin = lax.rem(here + length - k, length) * rows
+        low = place(begin + corner * part, half, cuts[c])
+        move(low, low, u_send.at[c, k], u_recv.at[c, k], partners[-1]).wait_recv()
+        high = place(begin + corner * part + half, half, cuts[c])
+        move(high, high, v_send.at[c, k], v_recv.at[c, k], partners[-2]).wait_recv()
+    for copy in started:
+        copy.wait_send()
+    own.wait()
+
+
+def spread(pieces):
+    width = sum(piece.shape[1] for piece in pieces)
+    padded = -(-width // 128) * 128
+    rows = pieces[0].shape[0]
+    if padded > width:
+        pieces = pieces + (jnp.zeros((rows, padded - width), pieces[0].dtype),)
+    shard = jnp.concatenate(pieces, axis=1)
+    length = lax.axis_size("sp")
+    edges = [128 * (padded // 128 * i // 3) for i in range(4)]
+    cuts = [(edges[i], edges[i + 1] - edges[i]) for i in range(3)]
+    return pl.pallas_call(
+        partial(spread_kernel, cuts),
+        out_shape=jax.ShapeDtypeStruct((length * rows, padded), shard.dtype),
+        in_specs=[pl.BlockSpec(memory_space=pl.ANY)],
+        out_specs=pl.BlockSpec(memory_space=pl.ANY),
+        scratch_shapes=[pltpu.SemaphoreType.DMA((3, length))] * 10 + [pltpu.SemaphoreType.DMA],
+        compiler_params=pltpu.CompilerParams(collective_id=0, has_side_effects=True),
+        cost_estimate=pl.CostEstimate(
+            flops=10**11, bytes_accessed=4 * length * rows * padded, transcendentals=0
+        ),
+    )(shard)
 
 
 def over_lanes(columns, width):
@@ -142,12 +255,18 @@
     def project(weight):
         return jnp.dot(normed, weight, preferred_element_type=jnp.float32).astype(jnp.bfloat16)
 
-    mixer_rows = project(gathered((weight_input, weight_write, weight_read, weight_step)))
-    glu_pair = project(gathered((weight_value, weight_sigmoid)))
+    front = project(
+        spread(
+            (weight_input, weight_write, weight_read, weight_value, weight_sigmoid, weight_step)
+        )
+    )
     gate_values = project(gathered((weight_gate,)))
     mixer_width = width + 2 * group_count * STATE
-    step_values = mixer_rows[:, mixer_width:]
-    mixer_rows = mixer_rows[:, :mixer_width]
+    channels = weight_value.shape[1]
+    mixer_rows = front[:, :mixer_width]
+    glu_pair = front[:, mixer_width : mixer_width + 2 * channels]
+    step_at = mixer_width + 2 * channels
+    step_values = front[:, step_at : step_at + head_count]
     short_rim = filter_input.shape[0] - 1
     long_rim = depth_filter.shape[0] - 1
     mixed = jax.nn.silu(
@@ -241,7 +360,6 @@
         jnp.repeat(skip_gain, HEAD_DIM)[None],
         output_gain[None],
     )
-    channels = weight_value.shape[1]
     glu_rows = (
         glu_pair[:, :channels].astype(jnp.float32)
         * jax.nn.sigmoid(glu_pair[:, channels:].astype(jnp.float32))

time: 475 us -> 345 us (0.73)
  waiting for transfers between devices: 343 us -> 13.5 us
  Pallas kernels: 13.7 us -> 195 us
  starting transfers between devices: 12.1 us -> 34.7 us
    all_gather x3 -> x1, waiting for transfers between devices: 269 us -> 0.01 us  [gathered(): return lax.all_gather(joined, ('sp', 'fs'), axis=0, tiled=True)]
    pallas_call x0 -> x1, Pallas kernels: none -> 181 us  [spread(): pl.pallas_call(partial(spread_kernel, cuts), out_shape=jax.ShapeDtypeStru...]
    all_gather x1, waiting for transfers between devices: 29.8 us -> 0.02 us  [per_device(): output_maps = lax.all_gather(piece, ('sp', 'fs'), axis=0, tiled=True)]
    ppermute x5, waiting for transfers between devices: 26.6 us -> 0.01 us  [passed_along(): return lax.ppermute(array, axis, pairs)]
    ppermute x5, starting transfers between devices: 11.9 us -> 34.6 us  [passed_along(): return lax.ppermute(array, axis, pairs)]
    concatenate x0 -> x1, local copies, waits for them, and re-layouts: none -> 6.64 us  [spread(): shard = jnp.concatenate(pieces, axis=1)]
    dot_general x3 -> x2, matrix products: 23.1 us -> 19.3 us  [project(): jnp.dot(normed, weight, preferred_element_type=jnp.float32)]
  transfers between devices with their start and end apart: 10 -> 8, of which waited for: 8 -> 1; matrix products, arithmetic and copies ran while one was open for 16% -> 20% of each run, Pallas kernels for 3% -> 57%
where the time goes in v2:
time: 345 us; the launch traced here: 344 us
  Pallas kernels  195 us (57%)
  starting transfers between devices  34.7 us (10%)
  local copies, waits for them, and re-layouts  29.5 us (9%)
  other arithmetic  28.6 us (8%)
  matrix products  26.2 us (8%)
  between operations  14.2 us (4%)
  waiting for transfers between devices  13.5 us (4%)
    pallas_call x1, Pallas kernels, spread(): pl.pallas_call(partial(spread_kernel, cuts), out_shape=jax.ShapeDtypeStru...  181 us
    ppermute x5, starting transfers between devices, passed_along(): return lax.ppermute(array, axis, pairs)  34.6 us
    dot_general x2, matrix products, project(): jnp.dot(normed, weight, preferred_element_type=jnp.float32)  19.3 us
    reduce_scatter x1, waiting for transfers between devices, per_device(): lax.psum_scatter(partial_rows, 'tp', scatter_dimension=0, tiled=True)  13.4 us
    reduce_sum x1, other arithmetic, per_device(): jnp.sum(filtered, axis=1)  9.99 us
    pallas_call x1, Pallas kernels, per_device(): pl.pallas_call(local_kernel, grid=(group_count,), in_specs=[wide, write_s...  7.28 us
    dot_general x4, matrix products, per_device(): jnp.dot(joined, output_maps[i], preferred_element_type=jnp.float32)  6.91 us
  transfers between devices with their start and end apart: 8, of which 1 were waited for; matrix products, arithmetic and copies ran while one was open for 20% of the time, Pallas kernels for 57%

profile of v2, /device:TPU:0, one launch (start us, length us, event | category | flops | bytes accessed | tf_op | source)
XLA Modules:
  0.0 343.8 jit_solution(1640805479330942384)
XLA Ops:
  6.6 1.2 copy-done
  8.6 1.1 constant_dynamic-slice_fusion
  10.8 6.6 %concatenate.25.shard_ref = bf16[512,4224]{1,0:T(8,128)(2,1)} concatenate(bf16[512,1024]{1,0:T(8,128)(2,1)S(1)} %copy-done.7, bf16[512,512]{1,0:T(8,128)(2,1)} %param.26, bf16[512,512]{1,0:T(8,128)(2,1)} %param.27, bf16[512,1024]{1,0:T(8,128)(2,1)S(1)} %copy-done.8, bf16[512,1024]{1,0:T(8,128)(2,1)S(1)} %copy-done.9, bf16[512,16]{1,0:T(8,128)(2,1)S(1)} %copy.45, ...), dimensions={1} | concatenate | bytes 8650752 | tf_op jit(solution)/shard_map/concatenate | solution.py:136
  17.5 180.9 %shard_map.208 = bf16[2048,4224]{1,0:T(8,128)(2,1)} custom-call(bf16[512,4224]{1,0:T(8,128)(2,1)} %concatenate.25.shard_ref), custom_call_target="tpu_custom_call" | custom-call | flops 99999997952 | bytes 34603008 | tf_op jit(solution)/shard_map/pallas_call | solution.py:140
  199.1 13.8 %convolution_convert_fusion = bf16[512,4224]{1,0:T(8,128)(2,1)S(1)} fusion(bf16[2048,4224]{1,0:T(8,128)(2,1)} %shard_map.208, bf16[1,512,2048]{2,1,0:T(8,128)(2,1)S(1)} %copy-done.5, f32[2048]{0:T(1024)S(1)} %copy-done.55, f32[512]{0:T(512)S(1)} %add_rsqrt_fusion.1), kind=kOutput, calls=%fused_computation | convolution fusion | flops 8864727040 | bytes 23734272 | tf_op jit(solution)/shard_map/dot_general | solution.py:256
  213.5 22.6 %collective-permute-start = (bf16[3,2048]{1,0:T(4,128)(2,1)}, bf16[3,2048]{1,0:T(4,128)(2,1)S(1)}, u32[]{:S(2)}, u32[]{:S(2)}) collective-permute-start(bf16[3,2048]{1,0:T(4,128)(2,1)} %slice.411), channel_id=1, source_target_pairs={{0,8},{8,16},{16,24},{1,9},{9,17},{17,25},{2,10},{10,18},{18,26},{... | collective-permute-start | bytes 36872 | tf_op jit(solution)/shard_map/ppermute | solution.py:19
  237.4 2.5 collective-permute-start.4
  240.1 1.1 bitcast_add_fusion
  244.1 1.3 copy.48
  245.4 1.9 fusion.63
  247.3 1.2 copy.49
  248.5 1.4 copy.50
  252.3 2.0 copy.53
  254.4 1.4 copy.56
  257.2 3.6 %multiply_convert_fusion.x_ref.write_ref.read_ref = bf16[512,2048]{1,0:T(8,128)(2,1)} fusion(f32[515,2048]{1,0:T(8,128)S(1)} %maximum_convert_fusion, f32[2048]{0:T(1024)S(1)} %bitcast.106, f32[2048]{0:T(1024)S(1)} %bitcast.107, f32[2048]{0:T(1024)S(1)} %bitcast.108, f32[2048]{0:T(1024)S(1)} %bitcast.105), kind=kLoop, calls=%fused_computation.13 | loop fusion | flops 12582912 | bytes 18907136 | tf_op jit(solution)/shard_map/convert_element_type | solution.py:278
  260.8 7.3 %shard_map.209 = (f32[512,1024]{1,0:T(8,128)}, f32[128,1024]{1,0:T(8,128)}) custom-call(bf16[512,2048]{1,0:T(8,128)(2,1)} %multiply_convert_fusion.x_ref.write_ref.read_ref, bf16[512,2048]{1,0:T(8,128)(2,1)} %multiply_convert_fusion.x_ref.write_ref.read_ref, bf16[512,2048]{1,0:T(8,128)(2,1)} %multiply_convert_fusion.x_ref.write_ref.read_ref, ...), custom_call_target="tpu_custom_call" | custom-call | flops 536870912 | bytes 4194304 | tf_op jit(solution)/shard_map/pallas_call | solution.py:304
  270.3 4.2 %collective-permute-start.3 = (bf16[144,1024]{1,0:T(8,128)(2,1)}, bf16[144,1024]{1,0:T(8,128)(2,1)}, u32[]{:S(2)}, u32[]{:S(2)}) collective-permute-start(bf16[144,1024]{1,0:T(8,128)(2,1)} %maximum_maximum_fusion), channel_id=1, source_target_pairs={{0,24},{1,25},{2,26},{3,27},{4,28},{5,29},{6,30},{7,31}} | collective-permute-start | bytes 884744 | tf_op jit(solution)/shard_map/ppermute | solution.py:19
  274.6 3.2 collective-permute-start.2
  277.7 2.0 collective-permute-start.1
  279.8 1.1 maximum_convert_fusion.1
  281.3 10.0 %fusion.67 = (f32[512]{0:T(512)S(1)}, f32[512]{0:T(512)S(1)}, f32[512,1024]{1,0:T(8,128)S(1)}) fusion(f32[542,1024]{1,0:T(8,128)S(1)} %maximum_convert_fusion.1, f32[1024]{0:T(1024)S(1)} %bitcast.124, f32[1024]{0:T(1024)S(1)} %bitcast.123, f32[1024]{0:T(1024)S(1)} %bitcast.122, f32[1024]{0:T(1024)S(1)} %bitcast.121, f32[1024]{0:T(1024)S(1)} %bitcast.120, ...), kind=kLoop, calls=%fused_computation.134 | loop fusion | flops 33553408 | bytes 67239936 | tf_op jit(solution)/shard_map/reduce_sum | solution.py:370
  291.3 2.5 all-reduce
  295.6 1.2 convert_element_type.120
  297.9 5.5 %convolution_convert_fusion.1.gate_ref = bf16[512,1024]{1,0:T(8,128)(2,1)} fusion(bf16[2048,1024]{1,0:T(8,128)(2,1)} %all-gather.3.cloned.1.call-done, bf16[1,512,2048]{2,1,0:T(8,128)(2,1)S(1)} %copy-done.6, f32[2048]{0:T(1024)S(1)} %copy-done.56, f32[512]{0:T(512)S(1)} %copy-done.52), kind=kOutput, calls=%fused_computation.88 | convolution fusion | flops 2152202240 | bytes 7350272 | tf_op jit(solution)/shard_map/dot_general | solution.py:256
  303.4 6.4 %shard_map.210 = bf16[512,1024]{1,0:T(8,128)(2,1)} custom-call(f32[512,1024]{1,0:T(8,128)} %get-tuple-element.7.y_ref, bf16[512,2048]{1,0:T(8,128)(2,1)} %multiply_convert_fusion.x_ref.write_ref.read_ref, bf16[512,2048]{1,0:T(8,128)(2,1)} %multiply_convert_fusion.x_ref.write_ref.read_ref, bf16[512,1024]{1,0:T(8,128)(2,1)} %convolution_convert_fusion.1.gate_ref, ...), custom_call_target="tpu_custom_call" | custom-call | flops 134217728 | bytes 5242880 | tf_op jit(solution)/shard_map/pallas_call | solution.py:344
  312.2 3.0 fusion.53
  316.2 1.3 fusion.50
  317.5 1.3 fusion.47
  318.8 1.3 fusion.44
  320.1 1.5 pad_maximum_fusion
  321.6 13.4 %reduce-scatter.2.cloned.1.call-done = bf16[256,2048]{0,1:T(8,128)(2,1)} async-done(((bf16[512,2048]{0,1:T(8,128)(2,1)}), bf16[256,2048]{0,1:T(8,128)(2,1)}) %reduce-scatter.2.cloned.1.call-update) | async-done | bytes 1048592 | tf_op jit(solution)/shard_map/reduce_scatter | solution.py:405
  335.1 2.3 copy.57
  (187 shorter events, 19.5 us)
Async XLA Ops:
  6.5 291.3 %all-gather.3.cloned.1.call-start = ((), (), s32[]{:S(2)}) async-start(), calls=%async_computation.1 | async-start | bytes 4456448 | tf_op jit(solution)/shard_map/all_gather | solution.py:39
  8.5 303.7 %all-gather.5.cloned.1.call-start = ((), (), s32[]{:S(2)}) async-start(), calls=%async_computation.2 | async-start | bytes 8912896 | tf_op jit(solution)/shard_map/all_gather | solution.py:388
  10.6 324.5 %reduce-scatter.2.cloned.1.call-start = ((), (), s32[]{:S(2)}) async-start(), calls=%async_computation.3 | async-start | bytes 3145728 | tf_op jit(solution)/shard_map/reduce_scatter | solution.py:405
  17.4 180.9 %copy-start.5 = (bf16[1,512,2048]{2,1,0:T(8,128)(2,1)S(1)}, bf16[1,512,2048]{2,1,0:T(8,128)(2,1)}, u32[]{:S(2)}) copy-start(bf16[1,512,2048]{2,1,0:T(8,128)(2,1)} %param.22) | copy-start | bytes 6291460
  199.1 13.8 %copy-start.51 = (f32[512]{0:T(512)}, f32[512]{0:T(512)S(1)}, u32[]{:S(2)}) copy-start(f32[512]{0:T(512)S(1)} %add_rsqrt_fusion.1) | copy-start | bytes 6148
  212.9 23.3 %copy-start.2 = (bf16[512,4224]{1,0:T(8,128)(2,1)}, bf16[512,4224]{1,0:T(8,128)(2,1)S(1)}, u32[]{:S(2)}) copy-start(bf16[512,4224]{1,0:T(8,128)(2,1)S(1)} %convolution_convert_fusion) | copy-start | bytes 12976132
  212.9 27.1 %copy-start.11 = (f32[1,16,512]{2,1,0:T(8,128)S(1)}, f32[1,16,512]{2,1,0:T(8,128)}, u32[]{:S(2)}) copy-start(f32[1,16,512]{2,1,0:T(8,128)} %param.39) | copy-start | bytes 98308
  212.9 27.2 %copy-start.57 = (f32[16]{0:T(128)S(1)}, f32[16]{0:T(128)}, u32[]{:S(2)}) copy-start(f32[16]{0:T(128)} %param.35) | copy-start | bytes 196
  212.9 27.2 %copy-start.50 = (f32[16]{0:T(128)S(1)}, f32[16]{0:T(128)}, u32[]{:S(2)}) copy-start(f32[16]{0:T(128)} %param.34) | copy-start | bytes 196
  213.5 28.5 %copy-start.46 = (bf16[4,1024]{1,0:T(4,128)(2,1)S(1)}, bf16[4,1024]{1,0:T(4,128)(2,1)}, u32[]{:S(2)}) copy-start(bf16[4,1024]{1,0:T(4,128)(2,1)} %param.31) | copy-start | bytes 24580
  213.5 28.5 %copy-start.48 = (bf16[4,512]{1,0:T(4,128)(2,1)S(1)}, bf16[4,512]{1,0:T(4,128)(2,1)}, u32[]{:S(2)}) copy-start(bf16[4,512]{1,0:T(4,128)(2,1)} %param.33) | copy-start | bytes 12292
  213.5 28.5 %copy-start.49 = (bf16[4,512]{1,0:T(4,128)(2,1)S(1)}, bf16[4,512]{1,0:T(4,128)(2,1)}, u32[]{:S(2)}) copy-start(bf16[4,512]{1,0:T(4,128)(2,1)} %param.32) | copy-start | bytes 12292
  213.5 28.5 %copy-start.10 = (bf16[31,1024]{1,0:T(8,128)(2,1)S(1)}, bf16[31,1024]{1,0:T(8,128)(2,1)}, u32[]{:S(2)}) copy-start(bf16[31,1024]{1,0:T(8,128)(2,1)} %param.40) | copy-start | bytes 190468
  213.5 43.1 %collective-permute-start = (bf16[3,2048]{1,0:T(4,128)(2,1)}, bf16[3,2048]{1,0:T(4,128)(2,1)S(1)}, u32[]{:S(2)}, u32[]{:S(2)}) collective-permute-start(bf16[3,2048]{1,0:T(4,128)(2,1)} %slice.411), channel_id=1, source_target_pairs={{0,8},{8,16},{16,24},{1,9},{9,17},{17,25},{2,10},{10,18},{18,26},{... | collective-permute-start | bytes 36872 | tf_op jit(solution)/shard_map/ppermute | solution.py:19
  237.4 42.4 %collective-permute-start.4 = (bf16[30,1024]{1,0:T(8,128)(2,1)}, bf16[30,1024]{1,0:T(8,128)(2,1)}, u32[]{:S(2)}, u32[]{:S(2)}) collective-permute-start(bf16[30,1024]{1,0:T(8,128)(2,1)} %slice.436), channel_id=1, source_target_pairs={{0,8},{8,16},{16,24},{1,9},{9,17},{17,25},{2,10},{10,18},{18,26},{... | collective-permute-start | bytes 184328 | tf_op jit(solution)/shard_map/ppermute | solution.py:19
  269.2 11.8 %copy-start.12 = (f32[1,1024]{1,0:T(1,128)S(1)}, f32[1,1024]{1,0:T(1,128)}, u32[]{:S(2)}) copy-start(f32[1,1024]{1,0:T(1,128)} %get-tuple-element.38) | copy-start | bytes 12292
  269.2 11.8 %copy-start.13 = (f32[1,1024]{1,0:T(1,128)S(1)}, f32[1,1024]{1,0:T(1,128)}, u32[]{:S(2)}) copy-start(f32[1,1024]{1,0:T(1,128)} %get-tuple-element.39) | copy-start | bytes 12292
  269.2 11.8 %copy-start.14 = (f32[1,1024]{1,0:T(1,128)S(1)}, f32[1,1024]{1,0:T(1,128)}, u32[]{:S(2)}) copy-start(f32[1,1024]{1,0:T(1,128)} %get-tuple-element.40) | copy-start | bytes 12292
  269.2 11.8 %copy-start.15 = (f32[1,1024]{1,0:T(1,128)S(1)}, f32[1,1024]{1,0:T(1,128)}, u32[]{:S(2)}) copy-start(f32[1,1024]{1,0:T(1,128)} %get-tuple-element.41) | copy-start | bytes 12292
  269.2 11.8 %copy-start.16 = (f32[1,1024]{1,0:T(1,128)S(1)}, f32[1,1024]{1,0:T(1,128)}, u32[]{:S(2)}) copy-start(f32[1,1024]{1,0:T(1,128)} %get-tuple-element.42) | copy-start | bytes 12292
  269.2 11.8 %copy-start.17 = (f32[1,1024]{1,0:T(1,128)S(1)}, f32[1,1024]{1,0:T(1,128)}, u32[]{:S(2)}) copy-start(f32[1,1024]{1,0:T(1,128)} %get-tuple-element.43) | copy-start | bytes 12292
  269.2 11.8 %copy-start.18 = (f32[1,1024]{1,0:T(1,128)S(1)}, f32[1,1024]{1,0:T(1,128)}, u32[]{:S(2)}) copy-start(f32[1,1024]{1,0:T(1,128)} %get-tuple-element.44) | copy-start | bytes 12292
  269.2 11.8 %copy-start.19 = (f32[1,1024]{1,0:T(1,128)S(1)}, f32[1,1024]{1,0:T(1,128)}, u32[]{:S(2)}) copy-start(f32[1,1024]{1,0:T(1,128)} %get-tuple-element.45) | copy-start | bytes 12292
  269.2 11.8 %copy-start.20 = (f32[1,1024]{1,0:T(1,128)S(1)}, f32[1,1024]{1,0:T(1,128)}, u32[]{:S(2)}) copy-start(f32[1,1024]{1,0:T(1,128)} %get-tuple-element.46) | copy-start | bytes 12292
  269.2 11.8 %copy-start.21 = (f32[1,1024]{1,0:T(1,128)S(1)}, f32[1,1024]{1,0:T(1,128)}, u32[]{:S(2)}) copy-start(f32[1,1024]{1,0:T(1,128)} %get-tuple-element.47) | copy-start | bytes 12292
  269.3 11.8 %copy-start.22 = (f32[1,1024]{1,0:T(1,128)S(1)}, f32[1,1024]{1,0:T(1,128)}, u32[]{:S(2)}) copy-start(f32[1,1024]{1,0:T(1,128)} %get-tuple-element.48) | copy-start | bytes 12292
  269.3 11.8 %copy-start.23 = (f32[1,1024]{1,0:T(1,128)S(1)}, f32[1,1024]{1,0:T(1,128)}, u32[]{:S(2)}) copy-start(f32[1,1024]{1,0:T(1,128)} %get-tuple-element.49) | copy-start | bytes 12292
  270.3 24.2 %collective-permute-start.3 = (bf16[144,1024]{1,0:T(8,128)(2,1)}, bf16[144,1024]{1,0:T(8,128)(2,1)}, u32[]{:S(2)}, u32[]{:S(2)}) collective-permute-start(bf16[144,1024]{1,0:T(8,128)(2,1)} %maximum_maximum_fusion), channel_id=1, source_target_pairs={{0,24},{1,25},{2,26},{3,27},{4,28},{5,29},{6,30},{7,31}} | collective-permute-start | bytes 884744 | tf_op jit(solution)/shard_map/ppermute | solution.py:19
  274.6 21.0 %collective-permute-start.2 = (bf16[144,1024]{1,0:T(8,128)(2,1)}, bf16[144,1024]{1,0:T(8,128)(2,1)}, u32[]{:S(2)}, u32[]{:S(2)}) collective-permute-start(bf16[144,1024]{1,0:T(8,128)(2,1)} %maximum_maximum_fusion), channel_id=1, source_target_pairs={{0,16},{8,24},{1,17},{9,25},{2,18},{10,26},{3,19},{11,27},{4,20},{... | collective-permute-start | bytes 884744 | tf_op jit(solution)/shard_map/ppermute | solution.py:19
  277.7 19.0 %collective-permute-start.1 = (bf16[144,1024]{1,0:T(8,128)(2,1)}, bf16[144,1024]{1,0:T(8,128)(2,1)S(1)}, u32[]{:S(2)}, u32[]{:S(2)}) collective-permute-start(bf16[144,1024]{1,0:T(8,128)(2,1)} %maximum_maximum_fusion), channel_id=1, source_target_pairs={{0,8},{8,16},{16,24},{1,9},{9,17},{17,25},{2,10},{10,18},{18,26},{... | collective-permute-start | bytes 884744 | tf_op jit(solution)/shard_map/ppermute | solution.py:19
  281.3 12.5 %copy-start.47 = (f32[1024]{0:T(1024)S(1)}, f32[1024]{0:T(1024)}, u32[]{:S(2)}) copy-start(f32[1024]{0:T(1024)} %param.41) | copy-start | bytes 12292
  321.6 15.7 %copy-start.1 = (bf16[512,1024]{1,0:T(8,128)(2,1)S(1)}, bf16[512,1024]{1,0:T(8,128)(2,1)}, u32[]{:S(2)}) copy-start(bf16[512,1024]{1,0:T(8,128)(2,1)} %param.24) | copy-start | bytes 3145732
  (35 other events, 288.8 us)
Sparse Core Ops, SparseCore 0:
  10.1 134.1 all-gather.2
  147.1 131.4 all-gather.4
  321.7 13.2 reduce-scatter.1
